TPU v7x, 32 devices: a whole 2x2x4 slice. The times are simulated.
32 devices in a mesh: grp: 2 (over y), fs: 4 (over z), tp: 4 (over x, core).
Axes of the slice: x: 2, y: 2, z: 4, core: 2. Of those that a mesh axis runs over, the one named last changes fastest.
Arguments:
- tokens: bfloat16 [2048, 2048], P(('grp', 'fs'), 'tp'), parts along dimension 0, may hold values from -6 to 6
- recurrent_norm_gain: float32 [2048], replicated, may hold values from 0.1 to 1.9
- feedforward_norm_gain: float32 [2048], replicated, may hold values from 0.1 to 1.9
- gate_projection_weight: bfloat16 [2048, 2048], P('fs', 'tp'), may hold values from -0.125 to 0.125
- recurrent_projection_weight: bfloat16 [2048, 2048], P('fs', 'tp'), may hold values from -0.125 to 0.125
- convolution_kernel: bfloat16 [4, 2048], P(None, 'tp'), may hold values from -3 to 3
- decay_gate_matrix: bfloat16 [16, 128, 128], P('tp'), may hold values from -0.5 to 0.5
- input_gate_matrix: bfloat16 [16, 128, 128], P('tp'), may hold values from -0.5 to 0.5
- base_decay_logit: float32 [2048], P('tp'), may hold values from 3 to 9
- extra_log_decay: float32 [2048], P(('grp', 'fs')), parts along dimension 0, may hold values from -0.7 to 0
- output_projection_weight: bfloat16 [2048, 2048], P('tp', 'fs'), may hold values from -0.125 to 0.125
- up_projection_weight: bfloat16 [2048, 8192], P('fs', 'tp'), may hold values from -0.125 to 0.125
- down_projection_weight: bfloat16 [8192, 2048], P('tp', 'fs'), may hold values from -0.0625 to 0.0625
Outputs:
- layer_out: bfloat16 [2048, 2048], P(('grp', 'fs'), 'tp'), parts along dimension 0
There are 2 independent parts, one for each index of `grp`. A program takes and returns all parts, laid end to end along the dimension named above; an argument that names none is the same for every part. Nothing has to cross between parts.
All inputs are finite; a program needn't handle non-finite values.
Results may differ from a plain program's by a relative error of at most 0.018.
Values may be sent and summed in bfloat16 or wider, within the bound.
A program may use at most 64 MiB of HBM per device.

v0:
```python
import functools

import jax
import jax.numpy as jnp
from jax import lax
from jax.experimental import pallas as pl
from jax.experimental.pallas import tpu as pltpu
from jax.sharding import PartitionSpec as P

MESH = pl.DeviceIdType.MESH


def rms_rows(values_in, norm_gain):
    values = values_in.astype(jnp.float32)
    inverse = lax.rsqrt(jnp.mean(values * values, axis=-1, keepdims=True) + 1e-06)
    return (values * inverse * norm_gain).astype(jnp.bfloat16)


def combine(earlier, later):
    return (earlier[0] * later[0], later[0] * earlier[1] + later[1])


def recurrent_state(
    recurrent_branch_rows,
    gate_branch_rows,
    convolution_kernel,
    decay_gate_matrix,
    input_gate_matrix,
    base_decay_logit,
    extra_log_decay,
):
    length = recurrent_branch_rows.shape[0]
    taps = convolution_kernel.shape[0]
    padded = jnp.pad(recurrent_branch_rows.astype(jnp.float32), ((taps - 1, 0), (0, 0)))
    conv_sum = jnp.zeros((length, recurrent_branch_rows.shape[1]), jnp.float32)
    for tap_index in range(taps):
        conv_sum = conv_sum + padded[tap_index : tap_index + length] * convolution_kernel[
            tap_index
        ].astype(jnp.float32)
    conv_rows = conv_sum.astype(jnp.bfloat16)
    blocks = decay_gate_matrix.shape[0]
    blocked = conv_rows.reshape(length, blocks, -1)
    recurrence_gate = jax.nn.sigmoid(
        jnp.einsum(
            "tni,nij->tnj", blocked, decay_gate_matrix, preferred_element_type=jnp.float32
        ).reshape(length, -1)
    )
    input_rate = jax.nn.sigmoid(
        jnp.einsum(
            "tni,nij->tnj", blocked, input_gate_matrix, preferred_element_type=jnp.float32
        ).reshape(length, -1)
    )
    decay_log_values = (
        -8.0 * jax.nn.softplus(-base_decay_logit) * recurrence_gate + extra_log_decay[:, None]
    )
    decay = jnp.exp(decay_log_values)
    drive = (
        jnp.sqrt(-jnp.expm1(2.0 * decay_log_values)) * input_rate * conv_rows.astype(jnp.float32)
    )
    _, hidden = lax.associative_scan(combine, (decay, drive), axis=0)
    return (hidden * gate_branch_rows.astype(jnp.float32)).astype(jnp.bfloat16)


def per_device(
    tokens,
    recurrent_norm_gain,
    feedforward_norm_gain,
    gate_projection_weight,
    recurrent_projection_weight,
    convolution_kernel,
    decay_gate_matrix,
    input_gate_matrix,
    base_decay_logit,
    extra_log_decay,
    output_projection_weight,
    up_projection_weight,
    down_projection_weight,
):
    whole_rows = lax.all_gather(tokens, "tp", axis=1, tiled=True)
    normed = rms_rows(whole_rows, recurrent_norm_gain)
    columns = normed
    gate_pre = jnp.dot(
        columns,
        lax.all_gather(gate_projection_weight, "fs", axis=0, tiled=True),
        preferred_element_type=jnp.float32,
    )
    recur_pre = jnp.dot(
        columns,
        lax.all_gather(recurrent_projection_weight, "fs", axis=0, tiled=True),
        preferred_element_type=jnp.float32,
    )
    gate_branch_rows = jax.nn.gelu(gate_pre).astype(jnp.bfloat16)
    recurrent_branch_rows = recur_pre.astype(jnp.bfloat16)
    mixed_output = recurrent_state(
        recurrent_branch_rows,
        gate_branch_rows,
        convolution_kernel,
        decay_gate_matrix,
        input_gate_matrix,
        base_decay_logit,
        extra_log_decay,
    )
    partials = jnp.dot(
        mixed_output,
        lax.all_gather(output_projection_weight, "fs", axis=1, tiled=True),
        preferred_element_type=jnp.float32,
    )
    residual = (
        tokens.astype(jnp.float32)
        + lax.psum_scatter(
            partials.astype(jnp.bfloat16), "tp", scatter_dimension=1, tiled=True
        ).astype(jnp.float32)
    ).astype(jnp.bfloat16)
    middle = lax.all_gather(residual, "tp", axis=1, tiled=True)
    channel_in = rms_rows(middle, feedforward_norm_gain)
    columns = channel_in
    upward = jnp.dot(
        columns,
        lax.all_gather(up_projection_weight, "fs", axis=0, tiled=True),
        preferred_element_type=jnp.float32,
    )
    positive = jnp.maximum(upward, 0.0)
    squared = (positive * positive).astype(jnp.bfloat16)
    down_terms = jnp.dot(
        squared,
        lax.all_gather(down_projection_weight, "fs", axis=1, tiled=True),
        preferred_element_type=jnp.float32,
    )
    summed_down = lax.psum_scatter(
        down_terms.astype(jnp.bfloat16), "tp", scatter_dimension=1, tiled=True
    ).astype(jnp.float32)
    return (residual.astype(jnp.float32) + summed_down).astype(jnp.bfloat16)


def steps_by_distance(count):
    return sorted(range(1, count), key=lambda step: (min(step, count - step), step))


def greet(count, place, row):
    barrier = pltpu.get_barrier_semaphore()
    peers = [{"fs": lax.rem(place + step, count)} for step in range(1, count)]
    peers += [{"tp": row ^ 1}, {"tp": row ^ 2}, {"grp": 1 - lax.axis_index("grp")}]
    for peer in peers:
        pl.semaphore_signal(barrier, inc=1, device_id=peer, device_id_type=MESH)
    pl.semaphore_wait(barrier, len(peers))


class Exchange:
    def __init__(self, count, axis, weight, joined, sems):
        self.count, self.axis, self.weight, self.joined, self.sems = (
            count, axis, weight, joined, sems
        )
        self.place, self.plane = lax.axis_index("fs"), lax.axis_index("grp")
        self.width = weight.shape[axis] // count
        self.depth = weight.shape[1 - axis]
        self.share = (self.depth if axis else self.width) // 2
        self.order = steps_by_distance(count)
        self.started = []

    def spot(self, rows, columns, row_step, column_step):
        return (
            pl.ds(pl.multiple_of(rows, row_step), self.share),
            pl.ds(pl.multiple_of(columns, column_step), self.width if self.axis else self.depth),
        )

    def leaving(self, owner, plane):
        half = plane * self.share
        if self.axis:
            return self.spot(half, owner * self.width, self.share, self.width)
        return self.spot(owner * self.width + half, 0, self.share, self.depth)

    def landing(self, source, plane):
        half = plane * self.share
        if self.axis:
            return self.spot(source * self.depth + half, 0, self.share, self.width)
        return self.spot(half, source * self.depth, self.share, self.depth)

    def copy(self, source, target, stage, step, peer):
        return pltpu.make_async_remote_copy(
            src_ref=source,
            dst_ref=target,
            send_sem=self.sems.at[stage, step],
            recv_sem=self.sems.at[stage + 1, step],
            device_id=peer,
            device_id_type=MESH,
        )

    def begin(self):
        for step in self.order:
            owner = lax.rem(self.place + step, self.count)
            moving = self.copy(
                self.weight.at[self.leaving(owner, self.plane)],
                self.joined.at[self.landing(self.place, self.plane)],
                0, step, {"fs": owner},
            )
            moving.start()
            self.started.append(moving)
        for plane in range(2):
            self.joined[self.landing(self.place, plane)] = self.weight[
                self.leaving(self.place, plane)
            ]

    def forward(self, step):
        source = lax.rem(self.place - step + self.count, self.count)
        peer = {"grp": 1 - self.plane}
        here = self.joined.at[self.landing(source, self.plane)]
        self.copy(here, here, 0, step, peer).wait_recv()
        moving = self.copy(here, here, 2, step, peer)
        moving.start()
        self.started.append(moving)

    def finish(self):
        for step in self.order:
            source = lax.rem(self.place - step + self.count, self.count)
            there = self.joined.at[self.landing(source, 1 - self.plane)]
            self.copy(there, there, 2, step, {"grp": 1 - self.plane}).wait_recv()
        for moving in self.started:
            moving.wait_send()


def joined_shape(weight, axis, count):
    shape = list(weight.shape)
    shape[axis] //= count
    shape[1 - axis] *= count
    return jax.ShapeDtypeStruct(tuple(shape), weight.dtype)


def gather_kernel(count, axes, *refs):
    held, send_z, send_x, send_c, arrived, moves, extra_sems = refs[-7:]
    own_ref, gain_ref, extra_ref = refs[:3]
    number = len(axes)
    out_ref, extra_out = refs[3 + number : 5 + number]
    exchanges = [
        Exchange(count, axis, refs[3 + k], refs[5 + number + k], moves.at[k])
        for k, axis in enumerate(axes)
    ]
    place, row = lax.axis_index("fs"), lax.axis_index("tp")
    across, beside, corner = row ^ 2, row ^ 1, row ^ 3
    length, width = own_ref.shape
    greet(count, place, row)

    def copy(source, at, send_sem, peer):
        return pltpu.make_async_remote_copy(
            src_ref=source,
            dst_ref=held.at[at[0], at[1]],
            send_sem=send_sem,
            recv_sem=arrived.at[at[0], at[1]],
            device_id=peer,
            device_id_type=MESH,
        )

    started = []

    def send(source, at, send_sem, peer):
        moving = copy(source, at, send_sem, peer)
        moving.start()
        started.append(moving)

    def wait(at):
        copy(held.at[at[0], at[1]], at, arrived.at[at[0], at[1]], {"tp": beside}).wait_recv()

    order = steps_by_distance(count)
    for step in order:
        send(own_ref, (place, row), send_z.at[step], {"fs": lax.rem(place + step, count)})
    send(own_ref, (place, row), send_x.at[0], {"tp": across})
    send(own_ref, (place, row), send_c.at[0, 0], {"tp": beside})
    for step in order:
        peer = lax.rem(place + step, count)
        moving = pltpu.make_async_remote_copy(
            src_ref=extra_ref.at[0],
            dst_ref=extra_out.at[place],
            send_sem=extra_sems.at[0, step],
            recv_sem=extra_sems.at[1, step],
            device_id={"fs": peer},
            device_id_type=MESH,
        )
        moving.start()
        started.append(moving)
    extra_out[place] = extra_ref[0]
    for exchange in exchanges:
        exchange.begin()
    held[place, row] = own_ref[...]
    for step in [0] + order:
        origin = lax.rem(place - step + count, count)
        if step:
            wait((origin, row))
            block = held.at[origin, row]
            send(block, (origin, row), send_x.at[step], {"tp": across})
            send(block, (origin, row), send_c.at[0, step], {"tp": beside})
        wait((origin, across))
        send(held.at[origin, across], (origin, across), send_c.at[1, step], {"tp": beside})
    for exchange in exchanges:
        for step in order:
            exchange.forward(step)
    tile = 64
    for step in [0] + order:
        origin = lax.rem(place - step + count, count)
        wait((origin, beside))
        wait((origin, corner))

        def normalise(index, carry):
            rows = pl.ds(pl.multiple_of(index * tile, tile), tile)
            parts = [held[origin, part, rows].astype(jnp.float32) for part in range(4)]
            total = sum(jnp.sum(part * part, axis=-1, keepdims=True) for part in parts)
            inverse = lax.rsqrt(total / (4 * width) + 1e-06)
            at = pl.ds(pl.multiple_of(origin * length + index * tile, tile), tile)
            for number, part in enumerate(parts):
                columns = pl.ds(number * width, width)
                out_ref[at, columns] = (part * inverse * gain_ref[:, columns]).astype(
                    out_ref.dtype
                )
            return carry

        lax.fori_loop(0, length // tile, normalise, 0)
    for exchange in exchanges:
        exchange.finish()
    for step in order:
        there = extra_out.at[lax.rem(place - step + count, count)]
        pltpu.make_async_remote_copy(
            src_ref=there,
            dst_ref=there,
            send_sem=extra_sems.at[0, step],
            recv_sem=extra_sems.at[1, step],
            device_id={"tp": beside},
            device_id_type=MESH,
        ).wait_recv()
    for moving in started:
        moving.wait_send()


def gather_normed(rows, norm_gain, extra, weights, axes, number):
    count = lax.axis_size("fs")
    length, width = rows.shape
    vmem = pl.BlockSpec(memory_space=pltpu.VMEM)
    dma = pltpu.SemaphoreType.DMA
    return pl.pallas_call(
        functools.partial(gather_kernel, count, axes),
        out_shape=[
            jax.ShapeDtypeStruct((count * length, 4 * width), rows.dtype),
            jax.ShapeDtypeStruct((count, 1, length), extra.dtype),
        ]
        + [joined_shape(weight, axis, count) for weight, axis in zip(weights, axes)],
        in_specs=[vmem] * (3 + len(axes)),
        out_specs=[vmem] * (2 + len(axes)),
        scratch_shapes=[
            pltpu.VMEM((count, 4, length, width), rows.dtype),
            dma((count,)),
            dma((count,)),
            dma((2, count)),
            dma((count, 4)),
            dma((len(axes), 4, count)),
            dma((2, count)),
        ],
        compiler_params=pltpu.CompilerParams(
            collective_id=number, has_side_effects=True, vmem_limit_bytes=32 * 2**20
        ),
        cost_estimate=pl.CostEstimate(flops=10**9, bytes_accessed=10**8, transcendentals=0),
    )(rows, norm_gain.reshape(1, -1), extra.reshape(1, 1, -1), *weights)


def scatter_kernel(count, axes, *refs):
    number = len(axes)
    terms_ref, base_ref = refs[:2]
    out_ref = refs[2 + number]
    from_core, to_x, from_x, to_z, from_z, send_c, recv_c, send_x, recv_x, send_z, recv_z = refs[
        3 + 2 * number : 14 + 2 * number
    ]
    exchanges = [
        Exchange(count, axis, refs[2 + k], refs[3 + number + k], refs[-1].at[k])
        for k, axis in enumerate(axes)
    ]
    place, row = lax.axis_index("fs"), lax.axis_index("tp")
    across, beside, corner = row ^ 2, row ^ 1, row ^ 3
    length, width = base_ref.shape
    greet(count, place, row)
    started = []

    def copy(source, target, send_sem, recv_sem, peer):
        return pltpu.make_async_remote_copy(
            src_ref=source,
            dst_ref=target,
            send_sem=send_sem,
            recv_sem=recv_sem,
            device_id=peer,
            device_id_type=MESH,
        )

    def send(*given):
        moving = copy(*given)
        moving.start()
        started.append(moving)

    def block(step, part):
        owner = lax.rem(place + step, count)
        return (
            pl.ds(pl.multiple_of(owner * length, length), length),
            pl.ds(pl.multiple_of(part * width, width), width),
        )

    def core_copy(step, side):
        part = corner if side else beside
        return (
            terms_ref.at[block(step, part)],
            from_core.at[side, step],
            send_c.at[side, step],
            recv_c.at[side, step],
            {"tp": beside},
        )

    def x_copy(step):
        return (to_x.at[step], from_x.at[step], send_x.at[step], recv_x.at[step], {"tp": across})

    def z_copy(step):
        peer = {"fs": lax.rem(place + step, count)}
        return (to_z.at[step], from_z.at[step], send_z.at[step], recv_z.at[step], peer)

    order = steps_by_distance(count)[::-1] + [0]
    for step in order:
        for side in (1, 0):
            send(*core_copy(step, side))
    wide = jnp.float32
    for exchange in exchanges:
        exchange.begin()
    for step in order:
        copy(*core_copy(step, 1)).wait_recv()
        mine = terms_ref[block(step, across)].astype(wide)
        to_x[step] = (mine + from_core[1, step].astype(wide)).astype(to_x.dtype)
        send(*x_copy(step))
    total = base_ref[...].astype(wide)
    summed = None
    for turn, step in enumerate(order):
        if turn:
            for exchange in exchanges:
                exchange.forward(exchange.order[turn - 1])
        copy(*core_copy(step, 0)).wait_recv()
        copy(*x_copy(step)).wait_recv()
        mine = terms_ref[block(step, row)].astype(wide) + from_core[0, step].astype(wide)
        mine = mine + from_x[step].astype(wide)
        if step:
            to_z[step] = mine.astype(to_z.dtype)
            send(*z_copy(step))
        else:
            summed = mine
    for step in order[:-1]:
        copy(*z_copy(step)).wait_recv()
        summed = summed + from_z[step].astype(wide)
    out_ref[...] = (total + summed).astype(out_ref.dtype)
    for exchange in exchanges:
        exchange.finish()
    for moving in started:
        moving.wait_send()


def scatter_added(terms, base, weights, axes, number):
    count = lax.axis_size("fs")
    vmem = pl.BlockSpec(memory_space=pltpu.VMEM)
    dma = pltpu.SemaphoreType.DMA
    blocks = pltpu.VMEM((count,) + base.shape, base.dtype)
    return pl.pallas_call(
        functools.partial(scatter_kernel, count, axes),
        out_shape=[jax.ShapeDtypeStruct(base.shape, base.dtype)]
        + [joined_shape(weight, axis, count) for weight, axis in zip(weights, axes)],
        in_specs=[vmem] * (2 + len(axes)),
        out_specs=[vmem] * (1 + len(axes)),
        scratch_shapes=[pltpu.VMEM((2, count) + base.shape, base.dtype)]
        + [blocks] * 4
        + [dma((2, count))] * 2
        + [dma((count,))] * 4
        + [dma((len(axes), 4, count)) for _ in axes[:1]],
        compiler_params=pltpu.CompilerParams(
            collective_id=number, has_side_effects=True, vmem_limit_bytes=24 * 2**20
        ),
        cost_estimate=pl.CostEstimate(flops=10**9, bytes_accessed=10**8, transcendentals=0),
    )(terms, base, *weights)


def recurrence_kernel(
    gate_ref, recur_ref, taps_ref, decay_map_ref, input_map_ref, rate_ref, extra_ref, out_ref
):
    wide = jnp.float32
    recur = recur_ref[...].astype(jnp.bfloat16).astype(wide)
    length = recur.shape[0]
    position = lax.broadcasted_iota(jnp.int32, recur.shape, 0)
    taps = taps_ref.shape[0]
    conv = recur * taps_ref[taps - 1 : taps].astype(wide)
    for tap in range(taps - 1):
        back = taps - 1 - tap
        earlier = jnp.where(position >= back, pltpu.roll(recur, back, 0), 0.0)
        conv = conv + earlier * taps_ref[tap : tap + 1].astype(wide)
    conv_rows = conv.astype(jnp.bfloat16)
    recur_gate = jax.nn.sigmoid(
        jnp.dot(conv_rows, decay_map_ref[0], preferred_element_type=wide)
    )
    input_rate = jax.nn.sigmoid(
        jnp.dot(conv_rows, input_map_ref[0], preferred_element_type=wide)
    )
    log_decay = rate_ref[...] * recur_gate + extra_ref[...]
    decay = jnp.exp(log_decay)
    spread = -jnp.tanh(log_decay) * (decay * decay + 1.0)
    drive = jnp.sqrt(spread) * input_rate * conv_rows.astype(wide)
    back = 1
    while back < length:
        inside = position >= back
        drive = drive + decay * jnp.where(inside, pltpu.roll(drive, back, 0), 0.0)
        if back * 2 < length:
            decay = decay * jnp.where(inside, pltpu.roll(decay, back, 0), 1.0)
        back *= 2
    gate_rows = jax.nn.gelu(gate_ref[...]).astype(jnp.bfloat16)
    out_ref[...] = (drive * gate_rows.astype(wide)).astype(out_ref.dtype)


def recurrence(both, taps, decay_map, input_map, rate, extra, count):
    blocks, size, _ = decay_map.shape
    length = both.shape[0] // count
    return pl.pallas_call(
        recurrence_kernel,
        grid=(count, blocks),
        out_shape=jax.ShapeDtypeStruct((count * length, blocks * size), jnp.bfloat16),
        in_specs=[
            pl.BlockSpec((length, size), lambda s, n: (s, n)),
            pl.BlockSpec((length, size), lambda s, n: (s, n + blocks)),
            pl.BlockSpec((taps.shape[0], size), lambda s, n: (0, n)),
            pl.BlockSpec((1, size, size), lambda s, n: (n, 0, 0)),
            pl.BlockSpec((1, size, size), lambda s, n: (n, 0, 0)),
            pl.BlockSpec((1, size), lambda s, n: (0, n)),
            pl.BlockSpec((length, 1), lambda s, n: (s, 0)),
        ],
        out_specs=pl.BlockSpec((length, size), lambda s, n: (s, n)),
        compiler_params=pltpu.CompilerParams(vmem_limit_bytes=24 * 2**20),
        cost_estimate=pl.CostEstimate(flops=10**8, bytes_accessed=10**7, transcendentals=10**6),
    )(both, both, taps, decay_map, input_map, rate.reshape(1, -1), extra.reshape(-1, 1))


def per_device_owned(
    tokens,
    recurrent_norm_gain,
    feedforward_norm_gain,
    gate_projection_weight,
    recurrent_projection_weight,
    convolution_kernel,
    decay_gate_matrix,
    input_gate_matrix,
    base_decay_logit,
    extra_log_decay,
    output_projection_weight,
    up_projection_weight,
    down_projection_weight,
):
    count, mine = lax.axis_size("fs"), lax.axis_index("fs")

    def own(value, axis):
        width = value.shape[axis] // count
        return lax.dynamic_slice_in_dim(value, mine * width, width, axis)

    depth = gate_projection_weight.shape[0]
    paired = [
        weight.reshape(depth, count, -1)
        for weight in (gate_projection_weight, recurrent_projection_weight)
    ]
    paired = jnp.concatenate(paired, axis=2).reshape(depth, -1)
    normed, extra, both_weight, out_weight = gather_normed(
        tokens,
        recurrent_norm_gain,
        extra_log_decay,
        (paired, output_projection_weight),
        (1, 0),
        1,
    )
    mixed = recurrence(
        jnp.dot(normed, both_weight, preferred_element_type=jnp.float32),
        own(convolution_kernel, 1),
        own(decay_gate_matrix, 0),
        own(input_gate_matrix, 0),
        -8.0 * jax.nn.softplus(-own(base_decay_logit, 0)),
        extra,
        count,
    )
    partials = jnp.dot(mixed, out_weight, preferred_element_type=jnp.float32)
    residual, up_weight = scatter_added(
        partials.astype(jnp.bfloat16), tokens, (up_projection_weight,), (1,), 2
    )
    channel_in, _, down_weight = gather_normed(
        residual, feedforward_norm_gain, extra_log_decay, (down_projection_weight,), (0,), 3
    )
    positive = jnp.maximum(
        jnp.dot(channel_in, up_weight, preferred_element_type=jnp.float32), 0.0
    )
    squared = (positive * positive).astype(jnp.bfloat16)
    down_terms = jnp.dot(squared, down_weight, preferred_element_type=jnp.float32)
    return scatter_added(down_terms.astype(jnp.bfloat16), residual, (), (), 4)[0]


def solution(mesh):
    placed = (
        P(("grp", "fs"), "tp"),
        P(),
        P(),
        P("fs", "tp"),
        P("fs", "tp"),
        P(None, "tp"),
        P("tp", None, None),
        P("tp", None, None),
        P("tp"),
        P(("grp", "fs")),
        P("tp", "fs"),
        P("fs", "tp"),
        P("tp", "fs"),
    )
    owners = mesh.shape["fs"] * mesh.shape["tp"]
    fitting = mesh.shape["tp"] == 4 and mesh.shape["grp"] == 2

    def run(*arrays):
        owned = fitting and arrays[6].shape[0] % owners == 0
        body = per_device_owned if owned else per_device
        return jax.shard_map(
            body, mesh=mesh, in_specs=placed, out_specs=P(("grp", "fs"), "tp"), check_vma=False
        )(*arrays)

    return run
```

profile of v0, /device:TPU:0, one launch (start us, length us, event | category | flops | bytes accessed | tf_op | source)
XLA Modules:
  0.0 222.9 jit_solution(4660365825304561256)
XLA Ops:
  0.0 0.0 copy-start
  0.0 0.8 fusion.1.rate_ref
  0.8 0.0 copy-done
  0.8 0.8 constant_dynamic-slice_fusion
  1.6 1.2 reshape.27
  2.8 1.2 reshape.28
  3.9 0.0 copy-start.3
  3.9 0.0 copy-start.7
  4.0 0.0 copy-start.8
  4.0 0.0 copy-start.10
  4.0 0.6 pad_maximum_fusion
  4.5 0.2 copy.15
  4.8 0.1 copy-done.3
  4.9 0.2 copy-done.7
  5.1 0.0 copy-done.8
  5.1 58.8 %shard_map.127 = (bf16[1024,2048]{1,0:T(8,128)(2,1)S(1)}, f32[4,1,256]{2,1,0:T(1,128)S(1)}, bf16[2048,256]{1,0:T(8,128)(2,1)S(1)}, bf16[128,2048]{1,0:T(8,128)(2,1)S(1)}) custom-call(bf16[256,512]{1,0:T(8,128)(2,1)S(1)} %copy-done.3, f32[1,2048]{1,0:T(1,128)S(1)} %bitcast.17, f32[1,1,256]{2,1,0:T(1,128)S(1)} %bitcast.19, bf16[512,1024]{1,0:T(8,128)(2,1)S(1)} %bitcast.15, ...), custom_call_target="tpu_custom_call" | custom-call | flops 1000000000 | bytes 100000000 | tf_op jit(solution)/shard_map/pallas_call | solution.py:336
  63.9 1.3 fusion.3.gate_ref.recur_ref
  65.2 0.2 copy.14.extra_ref
  65.4 2.0 shard_map.128
  67.4 0.0 copy-start.2
  67.4 1.2 convolution_convert_fusion.1.refs_0_
  68.7 0.3 copy-done.2
  69.0 42.5 %shard_map.129 = (bf16[256,512]{1,0:T(8,128)(2,1)S(1)}, bf16[2048,512]{1,0:T(8,128)(2,1)S(1)}) custom-call(bf16[1024,2048]{1,0:T(8,128)(2,1)S(1)} %convolution_convert_fusion.1.refs_0_, bf16[256,512]{1,0:T(8,128)(2,1)S(1)} %copy-done.3, bf16[512,2048]{1,0:T(8,128)(2,1)S(1)} %copy-done.2), custom_call_target="tpu_custom_call" | custom-call | flops 1000000000 | bytes 100000000 | tf_op jit(solution)/shard_map/pallas_call | solution.py:459
  111.5 1.3 copy-done.5
  112.9 0.0 copy-done.4
  112.9 58.9 %shard_map.130 = (bf16[1024,2048]{1,0:T(8,128)(2,1)S(1)}, f32[4,1,256]{2,1,0:T(1,128)}, bf16[512,2048]{1,0:T(8,128)(2,1)S(1)}) custom-call(bf16[256,512]{1,0:T(8,128)(2,1)S(1)} %get-tuple-element.17.refs_0_.refs_1_, f32[1,2048]{1,0:T(1,128)S(1)} %bitcast.18, f32[1,1,256]{2,1,0:T(1,128)S(1)} %bitcast.20, bf16[2048,512]{1,0:T(8,128)(2,1)S(1)} %copy-done.4), custom_call_target="tpu_custom_call" | custom-call | flops 1000000000 | bytes 100000000 | tf_op jit(solution)/shard_map/pallas_call | solution.py:336
  171.8 2.0 copy-done.11
  173.8 1.4 copy-done.12
  175.1 8.3 %convolution_convert_fusion.refs_0_ = bf16[1024,2048]{1,0:T(8,128)(2,1)} fusion(bf16[512,2048]{1,0:T(8,128)(2,1)} %copy-done.12, bf16[1024,2048]{1,0:T(8,128)(2,1)} %copy-done.11, bf16[2048,512]{1,0:T(8,128)(2,1)S(1)} %copy-done.6), kind=kOutput, calls=%fused_computation | convolution fusion | flops 4298637312 | bytes 12582912 | tf_op jit(solution)/shard_map/dot_general | solution.py:589
  183.4 2.2 copy-done.1
  185.6 36.6 %shard_map.131 = bf16[256,512]{1,0:T(8,128)(2,1)S(1)} custom-call(bf16[1024,2048]{1,0:T(8,128)(2,1)S(1)} %copy-done.1, bf16[256,512]{1,0:T(8,128)(2,1)S(1)} %get-tuple-element.17.refs_0_.refs_1_), custom_call_target="tpu_custom_call" | custom-call | flops 1000000000 | bytes 100000000 | tf_op jit(solution)/shard_map/pallas_call | solution.py:459
  222.2 0.7 copy.17
  (11 shorter events, 0.0 us)
Async XLA Ops:
  0.0 0.8 copy-start
  3.9 1.0 copy-start.3
  3.9 1.1 copy-start.7
  4.0 1.1 copy-start.8
  4.0 1.1 copy-start.10
  67.4 1.6 copy-start.2
  69.0 43.9 %copy-start.4 = (bf16[2048,512]{1,0:T(8,128)(2,1)S(1)}, bf16[2048,512]{1,0:T(8,128)(2,1)}, u32[]{:S(2)}) copy-start(bf16[2048,512]{1,0:T(8,128)(2,1)} %refs_3_.1) | copy-start | bytes 6291460
  69.0 43.9 %copy-start.9 = (f32[2048]{0:T(1024)S(1)}, f32[2048]{0:T(1024)}, u32[]{:S(2)}) copy-start(f32[2048]{0:T(1024)} %param.15) | copy-start | bytes 24580
  111.5 1.4 copy-start.5
  112.9 62.2 %copy-start.6 = (bf16[2048,512]{1,0:T(8,128)(2,1)S(1)}, bf16[2048,512]{1,0:T(8,128)(2,1)}, u32[]{:S(2)}) copy-start(bf16[2048,512]{1,0:T(8,128)(2,1)} %copy-done.5) | copy-start | bytes 6291460
  171.8 2.0 copy-start.11
  173.8 1.4 copy-start.12
  183.4 2.2 copy-start.1
where the time goes:
time: 224 us; the launch traced here: 223 us
  Pallas kernels  199 us (89%)
  local copies, waits for them, and re-layouts  11.8 us (5%)
  matrix products  10.8 us (5%)
    pallas_call x2, Pallas kernels, gather_normed(): pl.pallas_call(functools.partial(gather_kernel, count, axes), out_shape=[...  118 us
    pallas_call x2, Pallas kernels, scatter_added(): pl.pallas_call(functools.partial(scatter_kernel, count, axes), out_shape=...  79.1 us
    unnamed x28, local copies, waits for them, and re-layouts  8.45 us
    dot_general x1, matrix products, per_device_owned(): jnp.dot(squared, down_weight, preferred_element_type=jnp.float32)  8.27 us

commit v1 on v0

v1 whole, which is shorter than its diff:
```python
import functools

import jax
import jax.numpy as jnp
from jax import lax
from jax.experimental import pallas as pl
from jax.experimental.pallas import tpu as pltpu
from jax.sharding import PartitionSpec as P

MESH = pl.DeviceIdType.MESH


def rms_rows(values_in, norm_gain):
    values = values_in.astype(jnp.float32)
    inverse = lax.rsqrt(jnp.mean(values * values, axis=-1, keepdims=True) + 1e-06)
    return (values * inverse * norm_gain).astype(jnp.bfloat16)


def combine(earlier, later):
    return (earlier[0] * later[0], later[0] * earlier[1] + later[1])


def recurrent_state(
    recurrent_branch_rows,
    gate_branch_rows,
    convolution_kernel,
    decay_gate_matrix,
    input_gate_matrix,
    base_decay_logit,
    extra_log_decay,
):
    length = recurrent_branch_rows.shape[0]
    taps = convolution_kernel.shape[0]
    padded = jnp.pad(recurrent_branch_rows.astype(jnp.float32), ((taps - 1, 0), (0, 0)))
    conv_sum = jnp.zeros((length, recurrent_branch_rows.shape[1]), jnp.float32)
    for tap_index in range(taps):
        conv_sum = conv_sum + padded[tap_index : tap_index + length] * convolution_kernel[
            tap_index
        ].astype(jnp.float32)
    conv_rows = conv_sum.astype(jnp.bfloat16)
    blocks = decay_gate_matrix.shape[0]
    blocked = conv_rows.reshape(length, blocks, -1)
    recurrence_gate = jax.nn.sigmoid(
        jnp.einsum(
            "tni,nij->tnj", blocked, decay_gate_matrix, preferred_element_type=jnp.float32
        ).reshape(length, -1)
    )
    input_rate = jax.nn.sigmoid(
        jnp.einsum(
            "tni,nij->tnj", blocked, input_gate_matrix, preferred_element_type=jnp.float32
        ).reshape(length, -1)
    )
    decay_log_values = (
        -8.0 * jax.nn.softplus(-base_decay_logit) * recurrence_gate + extra_log_decay[:, None]
    )
    decay = jnp.exp(decay_log_values)
    drive = (
        jnp.sqrt(-jnp.expm1(2.0 * decay_log_values)) * input_rate * conv_rows.astype(jnp.float32)
    )
    _, hidden = lax.associative_scan(combine, (decay, drive), axis=0)
    return (hidden * gate_branch_rows.astype(jnp.float32)).astype(jnp.bfloat16)


def per_device(
    tokens,
    recurrent_norm_gain,
    feedforward_norm_gain,
    gate_projection_weight,
    recurrent_projection_weight,
    convolution_kernel,
    decay_gate_matrix,
    input_gate_matrix,
    base_decay_logit,
    extra_log_decay,
    output_projection_weight,
    up_projection_weight,
    down_projection_weight,
):
    whole_rows = lax.all_gather(tokens, "tp", axis=1, tiled=True)
    normed = rms_rows(whole_rows, recurrent_norm_gain)
    columns = normed
    gate_pre = jnp.dot(
        columns,
        lax.all_gather(gate_projection_weight, "fs", axis=0, tiled=True),
        preferred_element_type=jnp.float32,
    )
    recur_pre = jnp.dot(
        columns,
        lax.all_gather(recurrent_projection_weight, "fs", axis=0, tiled=True),
        preferred_element_type=jnp.float32,
    )
    gate_branch_rows = jax.nn.gelu(gate_pre).astype(jnp.bfloat16)
    recurrent_branch_rows = recur_pre.astype(jnp.bfloat16)
    mixed_output = recurrent_state(
        recurrent_branch_rows,
        gate_branch_rows,
        convolution_kernel,
        decay_gate_matrix,
        input_gate_matrix,
        base_decay_logit,
        extra_log_decay,
    )
    partials = jnp.dot(
        mixed_output,
        lax.all_gather(output_projection_weight, "fs", axis=1, tiled=True),
        preferred_element_type=jnp.float32,
    )
    residual = (
        tokens.astype(jnp.float32)
        + lax.psum_scatter(
            partials.astype(jnp.bfloat16), "tp", scatter_dimension=1, tiled=True
        ).astype(jnp.float32)
    ).astype(jnp.bfloat16)
    middle = lax.all_gather(residual, "tp", axis=1, tiled=True)
    channel_in = rms_rows(middle, feedforward_norm_gain)
    columns = channel_in
    upward = jnp.dot(
        columns,
        lax.all_gather(up_projection_weight, "fs", axis=0, tiled=True),
        preferred_element_type=jnp.float32,
    )
    positive = jnp.maximum(upward, 0.0)
    squared = (positive * positive).astype(jnp.bfloat16)
    down_terms = jnp.dot(
        squared,
        lax.all_gather(down_projection_weight, "fs", axis=1, tiled=True),
        preferred_element_type=jnp.float32,
    )
    summed_down = lax.psum_scatter(
        down_terms.astype(jnp.bfloat16), "tp", scatter_dimension=1, tiled=True
    ).astype(jnp.float32)
    return (residual.astype(jnp.float32) + summed_down).astype(jnp.bfloat16)

PIECES = 2
POOL = 157
TILE = 64


class Link:
    def __init__(self, pool):
        self.pool, self.started = pool, []

    def send(self, source, target, arrival, peer, only=None):
        moving = pltpu.make_async_remote_copy(
            src_ref=source,
            dst_ref=target,
            send_sem=self.pool.at[len(self.started)],
            recv_sem=arrival,
            device_id=peer,
            device_id_type=MESH,
        )
        self.started.append((moving, only))
        if only is None:
            moving.start()
        else:
            pl.when(only)(moving.start)

    def finish(self):
        for moving, only in self.started:
            if only is None:
                moving.wait_send()
            else:
                pl.when(only)(moving.wait_send)


def arrive(target, arrival, peer):
    pltpu.make_async_remote_copy(
        src_ref=target,
        dst_ref=target,
        send_sem=arrival,
        recv_sem=arrival,
        device_id=peer,
        device_id_type=MESH,
    ).wait_recv()


class Where:
    def __init__(self):
        self.place, self.row = lax.axis_index("fs"), lax.axis_index("tp")
        self.plane = lax.axis_index("grp")
        place = self.place
        self.near = place + 1 - 2 * lax.rem(place, 2)
        self.mid = 3 - place
        self.inner = lax.rem((place + 1) // 2, 2)
        self.is_inner, self.is_outer = self.inner == 1, self.inner == 0
        far = place // 2
        self.order = [place, self.near, 2 - far, 3 - 3 * far]
        self.across, self.beside, self.corner = self.row ^ 2, self.row ^ 1, self.row ^ 3


def greet(at):
    barrier = pltpu.get_barrier_semaphore()
    peers = [{"fs": spot} for spot in at.order[1:]]
    peers += [{"tp": at.beside}, {"tp": at.across}, {"grp": 1 - at.plane}]
    for peer in peers:
        pl.semaphore_signal(barrier, inc=1, device_id=peer, device_id_type=MESH)
    pl.semaphore_wait(barrier, len(peers))


class Gather:
    def __init__(self, at, link, own, held, arrived):
        self.at, self.link, self.own, self.held, self.arrived = at, link, own, held, arrived
        self.step = own.shape[0] // PIECES

    def piece(self, origin, part, number):
        return self.held.at[origin, part, pl.ds(number * self.step, self.step)]

    def send(self, source, origin, part, number, peer, only=None):
        self.link.send(
            source,
            self.piece(origin, part, number),
            self.arrived.at[origin, part, number],
            peer,
            only,
        )

    def wait(self, origin, part, number):
        arrive(
            self.piece(origin, part, number),
            self.arrived.at[origin, part, number],
            {"tp": self.at.beside},
        )

    def begin(self):
        at = self.at
        for number in range(PIECES):
            source = self.own.at[pl.ds(number * self.step, self.step)]
            self.send(source, at.place, at.row, number, {"fs": at.near})
            self.send(source, at.place, at.row, number, {"fs": at.mid}, at.is_inner)
            self.send(source, at.place, at.row, number, {"tp": at.across})
            self.send(source, at.place, at.row, number, {"tp": at.beside})

    def relay(self, k):
        at, origin = self.at, self.at.order[k]
        for number in range(PIECES):
            self.wait(origin, at.row, number)
            source = self.piece(origin, at.row, number)
            onward = {"fs": at.mid if k == 1 else at.near}
            self.send(source, origin, at.row, number, onward, at.is_inner)
            self.send(source, origin, at.row, number, {"tp": at.across})
            self.send(source, origin, at.row, number, {"tp": at.beside})

    def cross(self, k):
        at, origin = self.at, self.at.order[k]
        for number in range(PIECES):
            self.wait(origin, at.across, number)
            source = self.piece(origin, at.across, number)
            self.send(source, origin, at.across, number, {"tp": at.beside})

    def normalise(self, k, norm_gain, target):
        at, origin = self.at, self.at.order[k]
        for number in range(PIECES):
            self.wait(origin, at.beside, number)
            self.wait(origin, at.corner, number)
        length, width = self.own.shape
        parts_of = self.held.shape[1]

        def tile(index, carry):
            rows = pl.ds(pl.multiple_of(index * TILE, TILE), TILE)
            parts = [self.held[origin, p, rows].astype(jnp.float32) for p in range(parts_of)]
            total = sum(jnp.sum(part * part, axis=-1, keepdims=True) for part in parts)
            inverse = lax.rsqrt(total / (parts_of * width) + 1e-06)
            for number, part in enumerate(parts):
                columns = pl.ds(number * width, width)
                target[rows, columns] = (part * inverse * norm_gain[:, columns]).astype(
                    target.dtype
                )
            return carry

        lax.fori_loop(0, length // TILE, tile, 0)


class Scatter:
    def __init__(self, at, link, terms, from_core, to_x, from_x, to_z, from_z, sems):
        self.at, self.link, self.terms = at, link, terms
        self.from_core, self.to_x, self.from_x = from_core, to_x, from_x
        self.to_z, self.from_z = to_z, from_z
        self.core_sems, self.x_sems, self.z_sems = sems
        self.step = terms.shape[2] // PIECES

    def rows(self, number):
        return pl.ds(number * self.step, self.step)

    def core(self, k):
        at = self.at
        for side, part in ((1, at.corner), (0, at.beside)):
            self.link.send(
                self.terms.at[k, part],
                self.from_core.at[side, k],
                self.core_sems.at[side, k],
                {"tp": at.beside},
            )

    def x(self, k):
        at = self.at
        arrive(self.from_core.at[1, k], self.core_sems.at[1, k], {"tp": at.beside})
        for number in range(PIECES):
            rows = self.rows(number)
            mine = self.terms[k, at.across, rows].astype(jnp.float32)
            theirs = self.from_core[1, k, rows].astype(jnp.float32)
            self.to_x[k, rows] = (mine + theirs).astype(self.to_x.dtype)
            self.link.send(
                self.to_x.at[k, rows],
                self.from_x.at[k, rows],
                self.x_sems.at[k, number],
                {"tp": at.across},
            )

    def joined(self, k, number):
        rows = self.rows(number)
        mine = self.terms[k, self.at.row, rows].astype(jnp.float32)
        mine = mine + self.from_core[0, k, rows].astype(jnp.float32)
        return mine + self.from_x[k, rows].astype(jnp.float32)

    def taken(self, slot, number):
        rows = self.rows(number)
        arrive(
            self.from_z.at[slot, rows], self.z_sems.at[slot, number], {"fs": self.at.near}
        )
        return self.from_z[slot, rows].astype(jnp.float32)

    def ready(self, k, number):
        at, rows = self.at, self.rows(number)
        if not number:
            arrive(self.from_core.at[0, k], self.core_sems.at[0, k], {"tp": at.beside})
        arrive(self.from_x.at[k, rows], self.x_sems.at[k, number], {"tp": at.across})

    def z(self, k):
        at = self.at
        comes = {2: 0, 3: 1, 1: 4}[k]
        peer = at.near if k == 1 else at.near + at.inner * (at.mid - at.near)
        slot = {2: 3 * at.inner, 3: 1 + 3 * at.inner, 1: 2}[k]
        for number in range(PIECES):
            rows = self.rows(number)
            self.ready(k, number)

            @pl.when(at.is_inner)
            def _():
                total = self.joined(k, number) + self.taken(comes, number)
                self.to_z[k, rows] = total.astype(self.to_z.dtype)

            @pl.when(at.is_outer)
            def _():
                self.to_z[k, rows] = self.joined(k, number).astype(self.to_z.dtype)

            self.link.send(
                self.to_z.at[k, rows],
                self.from_z.at[slot, rows],
                self.z_sems.at[slot, number],
                {"fs": peer},
            )

    def own(self, base, target):
        at = self.at
        for number in range(PIECES):
            rows = self.rows(number)
            self.ready(0, number)

            @pl.when(at.is_inner)
            def _():
                total = self.joined(0, number) + self.taken(2, number) + self.taken(3, number)
                target[rows] = (base[rows].astype(jnp.float32) + total).astype(target.dtype)

            @pl.when(at.is_outer)
            def _():
                total = self.joined(0, number) + self.taken(2, number)
                target[rows] = (base[rows].astype(jnp.float32) + total).astype(target.dtype)


class Weights:
    def __init__(self, at, link, chunks, moves):
        self.at, self.link, self.chunks, self.moves = at, link, chunks, moves

    def spread(self, number, k):
        at, (leaving, landing) = self.at, self.chunks[number]
        owner = at.order[k]
        self.link.send(
            leaving(owner, at.plane),
            landing(at.place, at.plane),
            self.moves.at[number, 0, at.place],
            {"fs": owner},
        )

    def forward(self, number, k):
        at, (_, landing) = self.at, self.chunks[number]
        source, peer = at.order[k], {"grp": 1 - at.plane}
        here = landing(source, at.plane)
        arrive(here, self.moves.at[number, 0, source], peer)
        self.link.send(here, here, self.moves.at[number, 1, source], peer)

    def wait(self, number):
        at, (_, landing) = self.at, self.chunks[number]
        for source in at.order[1:]:
            arrive(
                landing(source, 1 - at.plane),
                self.moves.at[number, 1, source],
                {"grp": 1 - at.plane},
            )


def recurrence(both, taps, decay_map, input_map, rate, extra):
    wide = jnp.float32
    size = both.shape[1] // 2
    recur = both[:, size:].astype(jnp.bfloat16).astype(wide)
    length = recur.shape[0]
    position = lax.broadcasted_iota(jnp.int32, recur.shape, 0)
    count = taps.shape[0]
    conv = recur * taps[count - 1 : count].astype(wide)
    for tap in range(count - 1):
        back = count - 1 - tap
        earlier = jnp.where(position >= back, pltpu.roll(recur, back, 0), 0.0)
        conv = conv + earlier * taps[tap : tap + 1].astype(wide)
    conv_rows = conv.astype(jnp.bfloat16)
    recur_gate = jax.nn.sigmoid(jnp.dot(conv_rows, decay_map, preferred_element_type=wide))
    input_rate = jax.nn.sigmoid(jnp.dot(conv_rows, input_map, preferred_element_type=wide))
    log_decay = rate * recur_gate + extra
    decay = jnp.exp(log_decay)
    spread = -jnp.tanh(log_decay) * (decay * decay + 1.0)
    drive = jnp.sqrt(spread) * input_rate * conv_rows.astype(wide)
    back = 1
    while back < length:
        inside = position >= back
        drive = drive + decay * jnp.where(inside, pltpu.roll(drive, back, 0), 0.0)
        if back * 2 < length:
            decay = decay * jnp.where(inside, pltpu.roll(decay, back, 0), 1.0)
        back *= 2
    gate_rows = jax.nn.gelu(both[:, :size]).astype(jnp.bfloat16)
    return (drive * gate_rows.astype(wide)).astype(jnp.bfloat16)


def layer_kernel(
    tokens, gain_one, gain_two, taps, decay_map, input_map, logit, extra_own,
    gate, recur, outward, upward, downward, out,
    held_one, held_two, residual, normed, both_w, out_w, up_w, down_w, extra,
    terms, from_core, to_x, from_x, to_z, from_z,
    pool, arrived, core_sems, x_sems, z_sems, moves, extra_sems, local_sems,
):
    at = Where()
    greet(at)
    link = Link(pool)
    length, width = tokens.shape
    depth, size = gate.shape[0], taps.shape[1] // 4
    hidden = up_w.shape[1]
    half, place = depth // 2, at.place

    def spot(start, count, step):
        return pl.ds(pl.multiple_of(start, step), count)

    def by_rows(weight, joined, columns, first, pieces, piece):
        share = half // pieces

        def leaving(owner, plane):
            rows = spot(plane * half + piece * share, share, share)
            return weight.at[rows, spot(owner * columns, columns, columns)]

        def landing(source, plane):
            rows = spot(source * depth + plane * half + piece * share, share, share)
            return joined.at[rows, pl.ds(first, columns)]

        return leaving, landing

    def by_columns(weight, joined, rows_of, pieces, piece):
        share = rows_of // 2 // pieces

        def leaving(owner, plane):
            return weight.at[
                spot(owner * rows_of + plane * rows_of // 2 + piece * share, share, share)
            ]

        def landing(source, plane):
            rows = spot(plane * rows_of // 2 + piece * share, share, share)
            return joined.at[rows, spot(source * width, width, width)]

        return leaving, landing

    chunks = [
        by_rows(gate, both_w, size, 0, 1, 0),
        by_rows(recur, both_w, size, size, 1, 0),
        by_columns(outward, out_w, size, 1, 0),
        by_rows(upward, up_w, hidden, 0, 2, 0),
        by_rows(upward, up_w, hidden, 0, 2, 1),
        by_columns(downward, down_w, hidden, 2, 0),
        by_columns(downward, down_w, hidden, 2, 1),
    ]
    weights = Weights(at, link, chunks, moves)

    def spread(numbers, ks=(1, 2, 3)):
        for k in ks:
            for number in numbers:
                weights.spread(number, k)

    def forward(numbers, ks=(1, 2, 3)):
        for k in ks:
            for number in numbers:
                weights.forward(number, k)

    first = Gather(at, link, tokens, held_one, arrived.at[0])
    first.begin()
    spread((0, 1), (1,))
    for k in range(1, 4):
        link.send(
            extra_own.at[0], extra.at[place], extra_sems.at[place], {"fs": at.order[k]}
        )
    extra[place] = extra_own[0]
    local = []
    for number, (leaving, landing) in enumerate(chunks):
        for plane in range(2):
            moving = pltpu.make_async_copy(
                leaving(place, plane), landing(place, plane), local_sems.at[number, plane]
            )
            moving.start()
            local.append(moving)
    held_one[place, at.row] = tokens[...]
    first.relay(1)
    spread((0, 1), (2, 3))
    first.cross(0)
    first.relay(2)
    first.cross(1)
    forward((0, 1), (1,))
    first.relay(3)
    spread((2,))
    first.cross(2)
    spread((3,))
    for k in range(3):
        first.normalise(k, gain_one, normed.at[k])
    forward((0, 1), (2, 3))
    for source in at.order[1:]:
        arrive(extra.at[source], extra_sems.at[source], {"fs": at.near})
    first.cross(3)
    forward((2,))
    for moving in local:
        moving.wait()
    for number in range(3):
        weights.wait(number)

    own_taps = taps[:, spot(place * size, size, size)]
    own_logit = logit[:, spot(place * size, size, size)]
    rate = -8.0 * (
        jnp.maximum(-own_logit, 0.0) + jnp.log1p(jnp.exp(-jnp.abs(own_logit)))
    )

    def mix(k):
        both = jnp.dot(normed[k], both_w[...], preferred_element_type=jnp.float32)
        added = jnp.transpose(jnp.broadcast_to(extra[at.order[k]], (size, length)))
        mixed = recurrence(both, own_taps, decay_map[place], input_map[place], rate, added)
        for part in range(4):
            terms[0, k, part] = jnp.dot(
                mixed, out_w[:, pl.ds(part * width, width)], preferred_element_type=jnp.float32
            ).astype(terms.dtype)

    def scatter(turn):
        return Scatter(
            at, link, terms.at[turn], from_core.at[turn], to_x.at[turn], from_x.at[turn],
            to_z.at[turn], from_z.at[turn],
            (core_sems.at[turn], x_sems.at[turn], z_sems.at[turn]),
        )

    summed = scatter(0)
    mix(2)
    summed.core(2)
    first.normalise(3, gain_one, normed.at[3])
    mix(3)
    summed.core(3)
    summed.x(2)
    mix(1)
    summed.core(1)
    summed.x(3)
    mix(0)
    summed.core(0)
    summed.x(1)
    summed.z(2)
    spread((4,), (1,))
    summed.x(0)
    summed.z(3)
    spread((4,), (2, 3))
    forward((3,))
    summed.z(1)
    spread((5,), (1,))
    summed.own(tokens, residual)

    second = Gather(at, link, residual, held_two, arrived.at[1])
    second.begin()
    spread((5,), (2, 3))
    held_two[place, at.row] = residual[...]
    second.relay(1)
    spread((6,), (1,))
    second.cross(0)
    second.relay(2)
    forward((4,))
    second.cross(1)
    second.relay(3)
    spread((6,), (2, 3))
    second.cross(2)
    for k in range(3):
        second.normalise(k, gain_two, normed.at[k])
    forward((5,))
    second.cross(3)
    for number in (3, 4):
        weights.wait(number)
    forward((6,))
    for number in (5, 6):
        weights.wait(number)

    def feed(k):
        raised = jnp.dot(normed[k], up_w[...], preferred_element_type=jnp.float32)
        positive = jnp.maximum(raised, 0.0)
        squared = (positive * positive).astype(jnp.bfloat16)
        for part in range(4):
            terms[1, k, part] = jnp.dot(
                squared, down_w[:, pl.ds(part * width, width)], preferred_element_type=jnp.float32
            ).astype(terms.dtype)

    last = scatter(1)
    feed(2)
    last.core(2)
    second.normalise(3, gain_two, normed.at[3])
    feed(3)
    last.core(3)
    last.x(2)
    feed(1)
    last.core(1)
    last.x(3)
    feed(0)
    last.core(0)
    last.x(1)
    last.z(2)
    last.x(0)
    last.z(3)
    last.z(1)
    last.own(residual, out)
    link.finish()


def per_device_owned(
    tokens,
    recurrent_norm_gain,
    feedforward_norm_gain,
    gate_projection_weight,
    recurrent_projection_weight,
    convolution_kernel,
    decay_gate_matrix,
    input_gate_matrix,
    base_decay_logit,
    extra_log_decay,
    output_projection_weight,
    up_projection_weight,
    down_projection_weight,
):
    length, width = tokens.shape
    depth, size = gate_projection_weight.shape[0], gate_projection_weight.shape[1] // 4
    hidden = up_projection_weight.shape[1] // 4
    kind, wide = tokens.dtype, jnp.float32
    vmem, anywhere = pl.BlockSpec(memory_space=pltpu.VMEM), pl.BlockSpec(memory_space=pltpu.HBM)
    dma, block = pltpu.SemaphoreType.DMA, (length, width)
    scratch = [
        ((4, 4) + block, kind),
        ((4, 4) + block, kind),
        (block, kind),
        ((4, length, 4 * width), kind),
        ((4 * depth, 2 * size), kind),
        ((size, 4 * width), kind),
        ((4 * depth, hidden), kind),
        ((hidden, 4 * width), kind),
        ((4, 1, length), wide),
        ((2, 4, 4) + block, kind),
        ((2, 2, 4) + block, kind),
        ((2, 4) + block, kind),
        ((2, 4) + block, kind),
        ((2, 4) + block, kind),
        ((2, 5) + block, kind),
    ]
    return pl.pallas_call(
        layer_kernel,
        out_shape=jax.ShapeDtypeStruct(block, kind),
        in_specs=[vmem] * 8 + [anywhere] * 5,
        out_specs=vmem,
        scratch_shapes=[pltpu.VMEM(*entry) for entry in scratch]
        + [
            dma((POOL,)),
            dma((2, 4, 4, PIECES)),
            dma((2, 2, 4)),
            dma((2, 4, PIECES)),
            dma((2, 5, PIECES)),
            dma((7, 2, 4)),
            dma((4,)),
            dma((7, 2)),
        ],
        compiler_params=pltpu.CompilerParams(
            collective_id=1, has_side_effects=True, vmem_limit_bytes=58 * 2**20
        ),
    )(
        tokens,
        recurrent_norm_gain.reshape(1, -1),
        feedforward_norm_gain.reshape(1, -1),
        convolution_kernel,
        decay_gate_matrix,
        input_gate_matrix,
        base_decay_logit.reshape(1, -1),
        extra_log_decay.reshape(1, 1, -1),
        gate_projection_weight,
        recurrent_projection_weight,
        output_projection_weight,
        up_projection_weight,
        down_projection_weight,
    )


def solution(mesh):
    placed = (
        P(("grp", "fs"), "tp"),
        P(),
        P(),
        P("fs", "tp"),
        P("fs", "tp"),
        P(None, "tp"),
        P("tp", None, None),
        P("tp", None, None),
        P("tp"),
        P(("grp", "fs")),
        P("tp", "fs"),
        P("fs", "tp"),
        P("tp", "fs"),
    )
    owners = mesh.shape["fs"] * mesh.shape["tp"]
    fitting = mesh.shape["tp"] == 4 and mesh.shape["grp"] == 2 and mesh.shape["fs"] == 4

    def run(*arrays):
        owned = fitting and arrays[6].shape[0] == owners
        body = per_device_owned if owned else per_device
        return jax.shard_map(
            body, mesh=mesh, in_specs=placed, out_specs=P(("grp", "fs"), "tp"), check_vma=False
        )(*arrays)

    return run
```

time: 224 us -> 183 us (0.82)
  Pallas kernels: 199 us -> 181 us
  matrix products: 10.8 us -> 0 us
  local copies, waits for them, and re-layouts: 11.8 us -> 1.67 us
    pallas_call x5 -> x1, Pallas kernels: 199 us -> 181 us  [per_device_owned(): pl.pallas_call(layer_kernel, out_shape=jax.ShapeDtypeStruct(block, kind),...]
    dot_general x3 -> x0, matrix products: 10.8 us -> none  [the longest x1 8.27 us: per_device_owned(): jnp.dot(squared, down_weight, preferred_element_type=jnp.float32)]
    unnamed x28 -> x1, local copies, waits for them, and re-layouts: 8.45 us -> 1.67 us
    reshape x3 -> x0, local copies, waits for them, and re-layouts: 2.55 us -> none  [the longest x2 2.33 us: per_device_owned(): weight.reshape(depth, count, -1)]
where the time goes in v1:
time: 183 us
  Pallas kernels  181 us (99%)
    pallas_call x1, Pallas kernels, per_device_owned(): pl.pallas_call(layer_kernel, out_shape=jax.ShapeDtypeStruct(block, kind),...  181 us

profile of v1, /device:TPU:0, one launch (start us, length us, event | category | flops | bytes accessed | tf_op | source)
XLA Modules:
  0.0 182.8 jit_solution(9273673218162173549)
XLA Ops:
  0.0 181.1 %shard_map.127 = bf16[256,512]{1,0:T(8,128)(2,1)} custom-call(bf16[256,512]{1,0:T(8,128)(2,1)} %tokens.1, f32[1,2048]{1,0:T(1,128)} %bitcast.4, f32[1,2048]{1,0:T(1,128)} %bitcast.5, bf16[4,512]{1,0:T(4,128)(2,1)} %taps.1, bf16[4,128,128]{2,1,0:T(8,128)(2,1)} %decay_map.1, bf16[4,128,128]{2,1,0:T(8,128)(2,1)} %input_map.1, f32[1,512]{1,0:T(1,128)} %bitcast.6, ...), custom_call_target="tpu_custom_call" | custom-call | tf_op jit(solution)/shard_map/pallas_call | solution.py:672
  181.1 1.7 copy.15

commit v2 on v1

--- a/solution.py
+++ b/solution.py
@@ -132,7 +132,9 @@
     return (residual.astype(jnp.float32) + summed_down).astype(jnp.bfloat16)
 
 PIECES = 2
-POOL = 157
+POOL = 125
+UP, DOWN = (3, 4), (5, 6)
+LIMIT = 58 * 2**20
 TILE = 64
 
 
@@ -185,6 +187,9 @@
         self.is_inner, self.is_outer = self.inner == 1, self.inner == 0
         far = place // 2
         self.order = [place, self.near, 2 - far, 3 - 3 * far]
+        near, other = self.near, self.order[2]
+        self.sooner = [place, near + self.inner * (other - near)]
+        self.sooner += [other + self.inner * (near - other), self.order[3]]
         self.across, self.beside, self.corner = self.row ^ 2, self.row ^ 1, self.row ^ 3
 
 
@@ -198,8 +203,9 @@
 
 
 class Gather:
-    def __init__(self, at, link, own, held, arrived):
+    def __init__(self, at, link, pair, own, held, arrived):
         self.at, self.link, self.own, self.held, self.arrived = at, link, own, held, arrived
+        self.pair = pair
         self.step = own.shape[0] // PIECES
 
     def piece(self, origin, part, number):
@@ -221,14 +227,17 @@
             {"tp": self.at.beside},
         )
 
-    def begin(self):
+    def begin(self, along=True, aside=True):
         at = self.at
         for number in range(PIECES):
             source = self.own.at[pl.ds(number * self.step, self.step)]
-            self.send(source, at.place, at.row, number, {"fs": at.near})
-            self.send(source, at.place, at.row, number, {"fs": at.mid}, at.is_inner)
-            self.send(source, at.place, at.row, number, {"tp": at.across})
-            self.send(source, at.place, at.row, number, {"tp": at.beside})
+            if along:
+                self.send(source, at.place, at.row, number, {"fs": at.near})
+                if not self.pair:
+                    self.send(source, at.place, at.row, number, {"fs": at.mid}, at.is_inner)
+            if aside:
+                self.send(source, at.place, at.row, number, {"tp": at.across})
+                self.send(source, at.place, at.row, number, {"tp": at.beside})
 
     def relay(self, k):
         at, origin = self.at, self.at.order[k]
@@ -236,7 +245,8 @@
             self.wait(origin, at.row, number)
             source = self.piece(origin, at.row, number)
             onward = {"fs": at.mid if k == 1 else at.near}
-            self.send(source, origin, at.row, number, onward, at.is_inner)
+            if not self.pair:
+                self.send(source, origin, at.row, number, onward, at.is_inner)
             self.send(source, origin, at.row, number, {"tp": at.across})
             self.send(source, origin, at.row, number, {"tp": at.beside})
 
@@ -271,7 +281,8 @@
 
 
 class Scatter:
-    def __init__(self, at, link, terms, from_core, to_x, from_x, to_z, from_z, sems):
+    def __init__(self, at, link, pair, terms, from_core, to_x, from_x, to_z, from_z, sems):
+        self.pair = pair
         self.at, self.link, self.terms = at, link, terms
         self.from_core, self.to_x, self.from_x = from_core, to_x, from_x
         self.to_z, self.from_z = to_z, from_z
@@ -328,6 +339,18 @@
     def z(self, k):
         at = self.at
         comes = {2: 0, 3: 1, 1: 4}[k]
+        if self.pair:
+            for number in range(PIECES):
+                rows = self.rows(number)
+                self.ready(k, number)
+                self.to_z[k, rows] = self.joined(k, number).astype(self.to_z.dtype)
+                self.link.send(
+                    self.to_z.at[k, rows],
+                    self.from_z.at[2, rows],
+                    self.z_sems.at[2, number],
+                    {"fs": at.near},
+                )
+            return
         peer = at.near if k == 1 else at.near + at.inner * (at.mid - at.near)
         slot = {2: 3 * at.inner, 3: 1 + 3 * at.inner, 1: 2}[k]
         for number in range(PIECES):
@@ -355,6 +378,10 @@
         for number in range(PIECES):
             rows = self.rows(number)
             self.ready(0, number)
+            if self.pair:
+                total = self.joined(0, number) + self.taken(2, number)
+                target[rows] = (base[rows].astype(jnp.float32) + total).astype(target.dtype)
+                continue
 
             @pl.when(at.is_inner)
             def _():
@@ -371,36 +398,57 @@
     def __init__(self, at, link, chunks, moves):
         self.at, self.link, self.chunks, self.moves = at, link, chunks, moves
 
-    def spread(self, number, k):
-        at, (leaving, landing) = self.at, self.chunks[number]
+    def spread(self, number, k, only):
+        at, (leaving, landing, extra) = self.at, self.chunks[number]
         owner = at.order[k]
+        if extra:
+            if k == 3 or k == 1 and only is at.is_inner:
+                return
+            only = at.is_outer if k == 1 else only
         self.link.send(
             leaving(owner, at.plane),
             landing(at.place, at.plane),
             self.moves.at[number, 0, at.place],
             {"fs": owner},
+            only,
         )
 
     def forward(self, number, k):
-        at, (_, landing) = self.at, self.chunks[number]
-        source, peer = at.order[k], {"grp": 1 - at.plane}
+        at, (_, landing, extra) = self.at, self.chunks[number]
+        source, peer = at.sooner[k], {"grp": 1 - at.plane}
         here = landing(source, at.plane)
-        arrive(here, self.moves.at[number, 0, source], peer)
-        self.link.send(here, here, self.moves.at[number, 1, source], peer)
+
+        def arrived():
+            arrive(here, self.moves.at[number, 0, source], peer)
+
+        only = at.is_inner if extra else None
+        if only is None:
+            arrived()
+        else:
+            pl.when(only)(arrived)
+        self.link.send(here, here, self.moves.at[number, 1, source], peer, only)
 
     def wait(self, number):
-        at, (_, landing) = self.at, self.chunks[number]
-        for source in at.order[1:]:
-            arrive(
-                landing(source, 1 - at.plane),
-                self.moves.at[number, 1, source],
-                {"grp": 1 - at.plane},
-            )
+        at, (_, landing, extra) = self.at, self.chunks[number]
+
+        def arrived():
+            for source in at.order[1:]:
+                arrive(
+                    landing(source, 1 - at.plane),
+                    self.moves.at[number, 1, source],
+                    {"grp": 1 - at.plane},
+                )
+
+        if extra:
+            pl.when(at.is_inner)(arrived)
+        else:
+            arrived()
 
 
 def recurrence(both, taps, decay_map, input_map, rate, extra):
     wide = jnp.float32
     size = both.shape[1] // 2
+    block = decay_map[0].shape[1]
     recur = both[:, size:].astype(jnp.bfloat16).astype(wide)
     length = recur.shape[0]
     position = lax.broadcasted_iota(jnp.int32, recur.shape, 0)
@@ -411,8 +459,17 @@
         earlier = jnp.where(position >= back, pltpu.roll(recur, back, 0), 0.0)
         conv = conv + earlier * taps[tap : tap + 1].astype(wide)
     conv_rows = conv.astype(jnp.bfloat16)
-    recur_gate = jax.nn.sigmoid(jnp.dot(conv_rows, decay_map, preferred_element_type=wide))
-    input_rate = jax.nn.sigmoid(jnp.dot(conv_rows, input_map, preferred_element_type=wide))
+
+    def mapped(matrix):
+        products = [
+            jnp.dot(
+                conv_rows[:, n * block : (n + 1) * block], matrix[n], preferred_element_type=wide
+            )
+            for n in range(size // block)
+        ]
+        return jax.nn.sigmoid(jnp.concatenate(products, axis=1))
+
+    recur_gate, input_rate = mapped(decay_map), mapped(input_map)
     log_decay = rate * recur_gate + extra
     decay = jnp.exp(log_decay)
     spread = -jnp.tanh(log_decay) * (decay * decay + 1.0)
@@ -431,7 +488,7 @@
 def layer_kernel(
     tokens, gain_one, gain_two, taps, decay_map, input_map, logit, extra_own,
     gate, recur, outward, upward, downward, out,
-    held_one, held_two, residual, normed, both_w, out_w, up_w, down_w, extra,
+    held_one, held_two, residual, normed, mixed, squared, both_w, out_w, up_w, down_w, extra,
     terms, from_core, to_x, from_x, to_z, from_z,
     pool, arrived, core_sems, x_sems, z_sems, moves, extra_sems, local_sems,
 ):
@@ -439,102 +496,107 @@
     greet(at)
     link = Link(pool)
     length, width = tokens.shape
-    depth, size = gate.shape[0], taps.shape[1] // 4
-    hidden = up_w.shape[1]
+    depth, size = gate.shape[0], taps.shape[1] // 2
+    most = up_w.shape[1]
+    least = upward.shape[1] // 2 - most
     half, place = depth // 2, at.place
 
     def spot(start, count, step):
         return pl.ds(pl.multiple_of(start, step), count)
 
-    def by_rows(weight, joined, columns, first, pieces, piece):
-        share = half // pieces
-
+    def by_rows(weight, joined, columns, first, begins, extra=False):
         def leaving(owner, plane):
-            rows = spot(plane * half + piece * share, share, share)
-            return weight.at[rows, spot(owner * columns, columns, columns)]
+            return weight.at[spot(plane * half, half, half), spot(begins(owner), columns, 128)]
 
         def landing(source, plane):
-            rows = spot(source * depth + plane * half + piece * share, share, share)
+            rows = spot(source * depth + plane * half, half, half)
             return joined.at[rows, pl.ds(first, columns)]
 
-        return leaving, landing
-
-    def by_columns(weight, joined, rows_of, pieces, piece):
-        share = rows_of // 2 // pieces
+        return leaving, landing, extra
+
+    def by_columns(weight, joined, rows_of, first, begins, extra=False):
+        share = rows_of // 2
 
         def leaving(owner, plane):
-            return weight.at[
-                spot(owner * rows_of + plane * rows_of // 2 + piece * share, share, share)
-            ]
+            return weight.at[spot(begins(owner) + plane * share, share, 64)]
 
         def landing(source, plane):
-            rows = spot(plane * rows_of // 2 + piece * share, share, share)
+            rows = spot(first + plane * share, share, 64)
             return joined.at[rows, spot(source * width, width, width)]
 
-        return leaving, landing
+        return leaving, landing, extra
+
+    def of_pair(owner):
+        return lax.rem(owner, 2) * size
+
+    def basic(owner):
+        return owner * least + (owner + 1) // 3 * (most - least) + owner // 3 * (most - least)
+
+    def further(owner):
+        return basic(owner) + least
 
     chunks = [
-        by_rows(gate, both_w, size, 0, 1, 0),
-        by_rows(recur, both_w, size, size, 1, 0),
-        by_columns(outward, out_w, size, 1, 0),
-        by_rows(upward, up_w, hidden, 0, 2, 0),
-        by_rows(upward, up_w, hidden, 0, 2, 1),
-        by_columns(downward, down_w, hidden, 2, 0),
-        by_columns(downward, down_w, hidden, 2, 1),
+        by_rows(gate, both_w, size, 0, of_pair),
+        by_rows(recur, both_w, size, size, of_pair),
+        by_columns(outward, out_w, size, 0, of_pair),
+        by_rows(upward, up_w, least, 0, basic),
+        by_rows(upward, up_w, most - least, least, further, True),
+        by_columns(downward, down_w, least, 0, basic),
+        by_columns(downward, down_w, most - least, least, further, True),
     ]
     weights = Weights(at, link, chunks, moves)
 
-    def spread(numbers, ks=(1, 2, 3)):
+    def spread(numbers, ks=(1, 2, 3), only=None):
         for k in ks:
             for number in numbers:
-                weights.spread(number, k)
+                weights.spread(number, k, only)
 
     def forward(numbers, ks=(1, 2, 3)):
         for k in ks:
             for number in numbers:
                 weights.forward(number, k)
 
-    first = Gather(at, link, tokens, held_one, arrived.at[0])
+    first = Gather(at, link, True, tokens, held_one, arrived.at[0])
+    spread((0, 1), (1,))
     first.begin()
-    spread((0, 1), (1,))
-    for k in range(1, 4):
-        link.send(
-            extra_own.at[0], extra.at[place], extra_sems.at[place], {"fs": at.order[k]}
-        )
+    spread((0, 1), (2, 3))
+    link.send(extra_own.at[0], extra.at[place], extra_sems.at[place], {"fs": at.near})
     extra[place] = extra_own[0]
     local = []
-    for number, (leaving, landing) in enumerate(chunks):
+    for number, (leaving, landing, extra_part) in enumerate(chunks):
         for plane in range(2):
             moving = pltpu.make_async_copy(
                 leaving(place, plane), landing(place, plane), local_sems.at[number, plane]
             )
-            moving.start()
-            local.append(moving)
+            local.append((moving, extra_part))
+            if extra_part:
+                pl.when(at.is_inner)(moving.start)
+            else:
+                moving.start()
     held_one[place, at.row] = tokens[...]
+    first.cross(0)
+    first.normalise(0, gain_one, normed.at[0])
+    forward((0, 1), (1,))
     first.relay(1)
-    spread((0, 1), (2, 3))
-    first.cross(0)
-    first.relay(2)
+    spread((2,))
+    forward((0, 1), (2,))
     first.cross(1)
-    forward((0, 1), (1,))
-    first.relay(3)
-    spread((2,))
-    first.cross(2)
-    spread((3,))
-    for k in range(3):
-        first.normalise(k, gain_one, normed.at[k])
-    forward((0, 1), (2, 3))
-    for source in at.order[1:]:
-        arrive(extra.at[source], extra_sems.at[source], {"fs": at.near})
-    first.cross(3)
-    forward((2,))
-    for moving in local:
-        moving.wait()
-    for number in range(3):
+    first.normalise(1, gain_one, normed.at[1])
+    arrive(extra.at[at.near], extra_sems.at[at.near], {"fs": at.near})
+    for moving, extra_part in local:
+        if extra_part:
+            pl.when(at.is_inner)(moving.wait)
+        else:
+            moving.wait()
+    forward((0, 1), (3,))
+    forward((2,), (1,))
+    spread(UP)
+    for number in range(2):
         weights.wait(number)
-
-    own_taps = taps[:, spot(place * size, size, size)]
-    own_logit = logit[:, spot(place * size, size, size)]
+    side = lax.rem(place, 2)
+    blocks = size // decay_map.shape[1]
+    own_taps = taps[:, spot(side * size, size, size)]
+    own_logit = logit[:, spot(side * size, size, size)]
     rate = -8.0 * (
         jnp.maximum(-own_logit, 0.0) + jnp.log1p(jnp.exp(-jnp.abs(own_logit)))
     )
@@ -542,90 +604,118 @@
     def mix(k):
         both = jnp.dot(normed[k], both_w[...], preferred_element_type=jnp.float32)
         added = jnp.transpose(jnp.broadcast_to(extra[at.order[k]], (size, length)))
-        mixed = recurrence(both, own_taps, decay_map[place], input_map[place], rate, added)
+        maps = [
+            [matrix[side * blocks + n] for n in range(blocks)] for matrix in (decay_map, input_map)
+        ]
+        mixed[k] = recurrence(both, own_taps, *maps, rate, added)
+
+    def project(k):
         for part in range(4):
             terms[0, k, part] = jnp.dot(
-                mixed, out_w[:, pl.ds(part * width, width)], preferred_element_type=jnp.float32
+                mixed[k], out_w[:, pl.ds(part * width, width)], preferred_element_type=jnp.float32
             ).astype(terms.dtype)
 
     def scatter(turn):
         return Scatter(
-            at, link, terms.at[turn], from_core.at[turn], to_x.at[turn], from_x.at[turn],
+            at, link, not turn, terms.at[turn], from_core.at[turn], to_x.at[turn], from_x.at[turn],
             to_z.at[turn], from_z.at[turn],
             (core_sems.at[turn], x_sems.at[turn], z_sems.at[turn]),
         )
 
     summed = scatter(0)
-    mix(2)
-    summed.core(2)
-    first.normalise(3, gain_one, normed.at[3])
-    mix(3)
-    summed.core(3)
-    summed.x(2)
     mix(1)
+    forward((2,), (2,))
+    mix(0)
+    forward((2,), (3,))
+    weights.wait(2)
+    project(1)
     summed.core(1)
-    summed.x(3)
-    mix(0)
+    project(0)
     summed.core(0)
     summed.x(1)
-    summed.z(2)
-    spread((4,), (1,))
     summed.x(0)
-    summed.z(3)
-    spread((4,), (2, 3))
-    forward((3,))
     summed.z(1)
-    spread((5,), (1,))
+    forward(UP[:1])
     summed.own(tokens, residual)
 
-    second = Gather(at, link, residual, held_two, arrived.at[1])
+    second = Gather(at, link, False, residual, held_two, arrived.at[1])
     second.begin()
-    spread((5,), (2, 3))
     held_two[place, at.row] = residual[...]
+    forward(UP[1:], (1,))
     second.relay(1)
-    spread((6,), (1,))
+    spread(DOWN[:1], (2, 3), at.is_inner)
+    spread(DOWN[:1], (1, 2, 3), at.is_outer)
     second.cross(0)
     second.relay(2)
-    forward((4,))
+    spread(DOWN[:1], (1,), at.is_inner)
+    spread(DOWN[1:], (1, 2, 3), at.is_outer)
     second.cross(1)
+    second.normalise(0, gain_two, normed.at[0])
+    forward(UP[1:], (2, 3))
     second.relay(3)
-    spread((6,), (2, 3))
+    spread(DOWN[1:], (1, 2, 3), at.is_inner)
     second.cross(2)
-    for k in range(3):
-        second.normalise(k, gain_two, normed.at[k])
-    forward((5,))
+    forward(DOWN[:1], (1,))
+    second.normalise(1, gain_two, normed.at[1])
+    forward(DOWN[:1], (2, 3))
+    second.normalise(2, gain_two, normed.at[2])
     second.cross(3)
-    for number in (3, 4):
+    second.normalise(3, gain_two, normed.at[3])
+    for number in UP:
         weights.wait(number)
-    forward((6,))
-    for number in (5, 6):
-        weights.wait(number)
-
-    def feed(k):
-        raised = jnp.dot(normed[k], up_w[...], preferred_element_type=jnp.float32)
-        positive = jnp.maximum(raised, 0.0)
-        squared = (positive * positive).astype(jnp.bfloat16)
+    forward(DOWN[1:], (1,))
+    def raised(k, columns):
+        product = jnp.dot(normed[k], up_w[:, columns], preferred_element_type=jnp.float32)
+        positive = jnp.maximum(product, 0.0)
+        squared[k, :, columns] = (positive * positive).astype(squared.dtype)
+
+    def lift(k):
+        raised(k, pl.ds(0, least))
+
+        @pl.when(at.is_inner)
+        def _():
+            raised(k, pl.ds(least, most - least))
+
+    def lowered(k, count):
         for part in range(4):
             terms[1, k, part] = jnp.dot(
-                squared, down_w[:, pl.ds(part * width, width)], preferred_element_type=jnp.float32
+                squared[k, :, pl.ds(0, count)],
+                down_w[pl.ds(0, count), pl.ds(part * width, width)],
+                preferred_element_type=jnp.float32,
             ).astype(terms.dtype)
 
+    def lower(k):
+        @pl.when(at.is_inner)
+        def _():
+            lowered(k, most)
+
+        @pl.when(at.is_outer)
+        def _():
+            lowered(k, least)
+
     last = scatter(1)
-    feed(2)
+    lift(3)
+    lift(2)
+    forward(DOWN[1:], (2,))
+    lift(1)
+    lift(0)
+    forward(DOWN[1:], (3,))
+    for number in DOWN:
+        weights.wait(number)
+    lower(3)
+    last.core(3)
+    lower(2)
     last.core(2)
-    second.normalise(3, gain_two, normed.at[3])
-    feed(3)
-    last.core(3)
+    last.x(3)
+    lower(1)
+    last.core(1)
     last.x(2)
-    feed(1)
-    last.core(1)
-    last.x(3)
-    feed(0)
+    lower(0)
     last.core(0)
     last.x(1)
-    last.z(2)
     last.x(0)
     last.z(3)
+    last.z(2)
     last.z(1)
     last.own(residual, out)
     link.finish()
@@ -647,8 +737,9 @@
     down_projection_weight,
 ):
     length, width = tokens.shape
-    depth, size = gate_projection_weight.shape[0], gate_projection_weight.shape[1] // 4
+    depth, size = gate_projection_weight.shape[0], gate_projection_weight.shape[1] // 2
     hidden = up_projection_weight.shape[1] // 4
+    hidden += hidden // 4
     kind, wide = tokens.dtype, jnp.float32
     vmem, anywhere = pl.BlockSpec(memory_space=pltpu.VMEM), pl.BlockSpec(memory_space=pltpu.HBM)
     dma, block = pltpu.SemaphoreType.DMA, (length, width)
@@ -657,6 +748,8 @@
         ((4, 4) + block, kind),
         (block, kind),
         ((4, length, 4 * width), kind),
+        ((4, length, size), kind),
+        ((4, length, hidden), kind),
         ((4 * depth, 2 * size), kind),
         ((size, 4 * width), kind),
         ((4 * depth, hidden), kind),
@@ -686,7 +779,7 @@
             dma((7, 2)),
         ],
         compiler_params=pltpu.CompilerParams(
-            collective_id=1, has_side_effects=True, vmem_limit_bytes=58 * 2**20
+            collective_id=1, has_side_effects=True, vmem_limit_bytes=LIMIT
         ),
     )(
         tokens,

time: 183 us -> 148 us (0.81)
  Pallas kernels: 181 us -> 146 us
    pallas_call x1, Pallas kernels: 181 us -> 146 us  [per_device_owned(): pl.pallas_call(layer_kernel, out_shape=jax.ShapeDtypeStruct(block, kind),...]
where the time goes in v2:
time: 148 us
  Pallas kernels  146 us (99%)
  local copies, waits for them, and re-layouts  1.67 us (1%)
    pallas_call x1, Pallas kernels, per_device_owned(): pl.pallas_call(layer_kernel, out_shape=jax.ShapeDtypeStruct(block, kind),...  146 us

profile of v2, /device:TPU:0, one launch (start us, length us, event | category | flops | bytes accessed | tf_op | source)
XLA Modules:
  0.0 147.8 jit_solution(8788305539733790408)
XLA Ops:
  0.0 146.1 %shard_map.127 = bf16[256,512]{1,0:T(8,128)(2,1)} custom-call(bf16[256,512]{1,0:T(8,128)(2,1)} %tokens.1, f32[1,2048]{1,0:T(1,128)} %bitcast.4, f32[1,2048]{1,0:T(1,128)} %bitcast.5, bf16[4,512]{1,0:T(4,128)(2,1)} %taps.1, bf16[4,128,128]{2,1,0:T(8,128)(2,1)} %decay_map.1, bf16[4,128,128]{2,1,0:T(8,128)(2,1)} %input_map.1, f32[1,512]{1,0:T(1,128)} %bitcast.6, ...), custom_call_target="tpu_custom_call" | custom-call | tf_op jit(solution)/shard_map/pallas_call | solution.py:765
  146.1 1.7 %copy.15 = bf16[256,512]{1,0:T(8,128)(2,1)} copy(bf16[256,512]{1,0:T(8,128)(2,1)} %shard_map.127) | data formatting | bytes 524288

commit v3 on v2

--- a/solution.py
+++ b/solution.py
@@ -132,7 +132,7 @@
     return (residual.astype(jnp.float32) + summed_down).astype(jnp.bfloat16)
 
 PIECES = 2
-POOL = 125
+POOL = 56
 UP, DOWN = (3, 4), (5, 6)
 LIMIT = 58 * 2**20
 TILE = 64
@@ -142,11 +142,20 @@
     def __init__(self, pool):
         self.pool, self.started = pool, []
 
+    def drain(self, moving, only):
+        if only is None:
+            moving.wait_send()
+        else:
+            pl.when(only)(moving.wait_send)
+
     def send(self, source, target, arrival, peer, only=None):
+        turn = len(self.started)
+        if turn >= POOL:
+            self.drain(*self.started[turn - POOL])
         moving = pltpu.make_async_remote_copy(
             src_ref=source,
             dst_ref=target,
-            send_sem=self.pool.at[len(self.started)],
+            send_sem=self.pool.at[turn % POOL],
             recv_sem=arrival,
             device_id=peer,
             device_id_type=MESH,
@@ -158,11 +167,8 @@
             pl.when(only)(moving.start)
 
     def finish(self):
-        for moving, only in self.started:
-            if only is None:
-                moving.wait_send()
-            else:
-                pl.when(only)(moving.wait_send)
+        for moving, only in self.started[-POOL:]:
+            self.drain(moving, only)
 
 
 def arrive(target, arrival, peer):
@@ -413,7 +419,7 @@
             only,
         )
 
-    def forward(self, number, k):
+    def forward(self, number, k, only):
         at, (_, landing, extra) = self.at, self.chunks[number]
         source, peer = at.sooner[k], {"grp": 1 - at.plane}
         here = landing(source, at.plane)
@@ -421,7 +427,9 @@
         def arrived():
             arrive(here, self.moves.at[number, 0, source], peer)
 
-        only = at.is_inner if extra else None
+        if extra and only is at.is_outer:
+            return
+        only = at.is_inner if extra else only
         if only is None:
             arrived()
         else:
@@ -486,14 +494,27 @@
 
 
 def layer_kernel(
-    tokens, gain_one, gain_two, taps, decay_map, input_map, logit, extra_own,
-    gate, recur, outward, upward, downward, out,
+    tokens_from, gain_one_from, gain_two_from, taps_from, decay_map_from, input_map_from,
+    logit_from, extra_from, gate, recur, outward, upward, downward, out,
     held_one, held_two, residual, normed, mixed, squared, both_w, out_w, up_w, down_w, extra,
     terms, from_core, to_x, from_x, to_z, from_z,
-    pool, arrived, core_sems, x_sems, z_sems, moves, extra_sems, local_sems,
+    tokens, gain_one, gain_two, taps, decay_map, input_map, logit, extra_own,
+    small_sems, pool, arrived, core_sems, x_sems, z_sems, moves, extra_sems, local_sems,
 ):
     at = Where()
+    small = []
+    for number, (source, target) in enumerate(
+        (
+            (tokens_from, tokens), (extra_from, extra_own), (gain_one_from, gain_one),
+            (taps_from, taps), (decay_map_from, decay_map), (input_map_from, input_map),
+            (logit_from, logit), (gain_two_from, gain_two),
+        )
+    ):
+        small.append(pltpu.make_async_copy(source, target, small_sems.at[number]))
+        small[-1].start()
     greet(at)
+    for moving in small:
+        moving.wait()
     link = Link(pool)
     length, width = tokens.shape
     depth, size = gate.shape[0], taps.shape[1] // 2
@@ -551,12 +572,12 @@
             for number in numbers:
                 weights.spread(number, k, only)
 
-    def forward(numbers, ks=(1, 2, 3)):
+    def forward(numbers, ks=(1, 2, 3), only=None):
         for k in ks:
             for number in numbers:
-                weights.forward(number, k)
-
-    first = Gather(at, link, True, tokens, held_one, arrived.at[0])
+                weights.forward(number, k, only)
+
+    first = Gather(at, link, True, tokens, held_one, arrived)
     spread((0, 1), (1,))
     first.begin()
     spread((0, 1), (2, 3))
@@ -590,9 +611,9 @@
             moving.wait()
     forward((0, 1), (3,))
     forward((2,), (1,))
-    spread(UP)
     for number in range(2):
         weights.wait(number)
+    spread(UP)
     side = lax.rem(place, 2)
     blocks = size // decay_map.shape[1]
     own_taps = taps[:, spot(side * size, size, size)]
@@ -619,7 +640,7 @@
         return Scatter(
             at, link, not turn, terms.at[turn], from_core.at[turn], to_x.at[turn], from_x.at[turn],
             to_z.at[turn], from_z.at[turn],
-            (core_sems.at[turn], x_sems.at[turn], z_sems.at[turn]),
+            (core_sems, x_sems, z_sems),
         )
 
     summed = scatter(0)
@@ -635,35 +656,38 @@
     summed.x(1)
     summed.x(0)
     summed.z(1)
+    spread(DOWN[:1], (2, 3, 1), at.is_inner)
     forward(UP[:1])
+    spread(DOWN[:1], (1,), at.is_outer)
     summed.own(tokens, residual)
 
-    second = Gather(at, link, False, residual, held_two, arrived.at[1])
+    second = Gather(at, link, False, residual, held_two, arrived)
     second.begin()
+    spread(DOWN[1:], (1,), at.is_outer)
     held_two[place, at.row] = residual[...]
-    forward(UP[1:], (1,))
+    forward(UP[1:])
+    forward(DOWN[:1], (1,))
     second.relay(1)
-    spread(DOWN[:1], (2, 3), at.is_inner)
-    spread(DOWN[:1], (1, 2, 3), at.is_outer)
+    spread(DOWN[:1], (2, 3), at.is_outer)
+    spread(DOWN[1:], (2,), at.is_outer)
     second.cross(0)
     second.relay(2)
-    spread(DOWN[:1], (1,), at.is_inner)
-    spread(DOWN[1:], (1, 2, 3), at.is_outer)
+    spread(DOWN[1:], (2,), at.is_inner)
     second.cross(1)
+    forward(DOWN[:1], (2,))
     second.normalise(0, gain_two, normed.at[0])
-    forward(UP[1:], (2, 3))
     second.relay(3)
-    spread(DOWN[1:], (1, 2, 3), at.is_inner)
     second.cross(2)
-    forward(DOWN[:1], (1,))
+    forward(DOWN[:1], (3,))
+    forward(DOWN[1:], (2,))
     second.normalise(1, gain_two, normed.at[1])
-    forward(DOWN[:1], (2, 3))
     second.normalise(2, gain_two, normed.at[2])
     second.cross(3)
+    forward(DOWN[1:], (1,))
     second.normalise(3, gain_two, normed.at[3])
+    forward(DOWN[1:], (3,))
     for number in UP:
         weights.wait(number)
-    forward(DOWN[1:], (1,))
     def raised(k, columns):
         product = jnp.dot(normed[k], up_w[:, columns], preferred_element_type=jnp.float32)
         positive = jnp.maximum(product, 0.0)
@@ -696,10 +720,8 @@
     last = scatter(1)
     lift(3)
     lift(2)
-    forward(DOWN[1:], (2,))
     lift(1)
     lift(0)
-    forward(DOWN[1:], (3,))
     for number in DOWN:
         weights.wait(number)
     lower(3)
@@ -761,19 +783,28 @@
         ((2, 4) + block, kind),
         ((2, 4) + block, kind),
         ((2, 5) + block, kind),
+        (block, kind),
+        ((1, 4 * width), wide),
+        ((1, 4 * width), wide),
+        (convolution_kernel.shape, convolution_kernel.dtype),
+        (decay_gate_matrix.shape, decay_gate_matrix.dtype),
+        (input_gate_matrix.shape, input_gate_matrix.dtype),
+        ((1, base_decay_logit.shape[0]), wide),
+        ((1, 1, length), wide),
     ]
     return pl.pallas_call(
         layer_kernel,
         out_shape=jax.ShapeDtypeStruct(block, kind),
-        in_specs=[vmem] * 8 + [anywhere] * 5,
+        in_specs=[anywhere] * 13,
         out_specs=vmem,
         scratch_shapes=[pltpu.VMEM(*entry) for entry in scratch]
         + [
+            dma((8,)),
             dma((POOL,)),
-            dma((2, 4, 4, PIECES)),
-            dma((2, 2, 4)),
-            dma((2, 4, PIECES)),
-            dma((2, 5, PIECES)),
+            dma((4, 4, PIECES)),
+            dma((2, 4)),
+            dma((4, PIECES)),
+            dma((5, PIECES)),
             dma((7, 2, 4)),
             dma((4,)),
             dma((7, 2)),

time: 148 us -> 138 us (0.932)
  Pallas kernels: 146 us -> 136 us
    pallas_call x1, Pallas kernels: 146 us -> 136 us  [per_device_owned(): pl.pallas_call(layer_kernel, out_shape=jax.ShapeDtypeStruct(block, kind),...]
where the time goes in v3:
time: 138 us
  Pallas kernels  136 us (99%)
  local copies, waits for them, and re-layouts  1.67 us (1%)
    pallas_call x1, Pallas kernels, per_device_owned(): pl.pallas_call(layer_kernel, out_shape=jax.ShapeDtypeStruct(block, kind),...  136 us

profile of v3, /device:TPU:0, one launch (start us, length us, event | category | flops | bytes accessed | tf_op | source)
XLA Modules:
  0.0 137.5 jit_solution(8918168710959326187)
XLA Ops:
  0.0 135.9 %shard_map.127 = bf16[256,512]{1,0:T(8,128)(2,1)} custom-call(bf16[256,512]{1,0:T(8,128)(2,1)} %tokens_from.1, f32[1,2048]{1,0:T(1,128)} %bitcast.4, f32[1,2048]{1,0:T(1,128)} %bitcast.5, bf16[4,512]{1,0:T(4,128)(2,1)} %taps_from.1, bf16[4,128,128]{2,1,0:T(8,128)(2,1)} %decay_map_from.1, bf16[4,128,128]{2,1,0:T(8,128)(2,1)} %input_map_from.1, ...), custom_call_target="tpu_custom_call" | custom-call | tf_op jit(solution)/shard_map/pallas_call | solution.py:795
  135.9 1.7 %copy.15 = bf16[256,512]{1,0:T(8,128)(2,1)} copy(bf16[256,512]{1,0:T(8,128)(2,1)} %shard_map.127) | data formatting | bytes 524288

commit v4 on v3

--- a/solution.py
+++ b/solution.py
@@ -131,8 +131,8 @@
     ).astype(jnp.float32)
     return (residual.astype(jnp.float32) + summed_down).astype(jnp.bfloat16)
 
-PIECES = 2
-POOL = 56
+PIECES, SPLIT = 2, 2
+POOL = 40
 UP, DOWN = (3, 4), (5, 6)
 LIMIT = 58 * 2**20
 TILE = 64
@@ -293,7 +293,7 @@
         self.from_core, self.to_x, self.from_x = from_core, to_x, from_x
         self.to_z, self.from_z = to_z, from_z
         self.core_sems, self.x_sems, self.z_sems = sems
-        self.step = terms.shape[2] // PIECES
+        self.step = terms.shape[2] // SPLIT
 
     def rows(self, number):
         return pl.ds(number * self.step, self.step)
@@ -311,7 +311,7 @@
     def x(self, k):
         at = self.at
         arrive(self.from_core.at[1, k], self.core_sems.at[1, k], {"tp": at.beside})
-        for number in range(PIECES):
+        for number in range(SPLIT):
             rows = self.rows(number)
             mine = self.terms[k, at.across, rows].astype(jnp.float32)
             theirs = self.from_core[1, k, rows].astype(jnp.float32)
@@ -346,7 +346,7 @@
         at = self.at
         comes = {2: 0, 3: 1, 1: 4}[k]
         if self.pair:
-            for number in range(PIECES):
+            for number in range(SPLIT):
                 rows = self.rows(number)
                 self.ready(k, number)
                 self.to_z[k, rows] = self.joined(k, number).astype(self.to_z.dtype)
@@ -359,7 +359,7 @@
             return
         peer = at.near if k == 1 else at.near + at.inner * (at.mid - at.near)
         slot = {2: 3 * at.inner, 3: 1 + 3 * at.inner, 1: 2}[k]
-        for number in range(PIECES):
+        for number in range(SPLIT):
             rows = self.rows(number)
             self.ready(k, number)
 
@@ -381,7 +381,7 @@
 
     def own(self, base, target):
         at = self.at
-        for number in range(PIECES):
+        for number in range(SPLIT):
             rows = self.rows(number)
             self.ready(0, number)
             if self.pair:
@@ -599,9 +599,9 @@
     first.normalise(0, gain_one, normed.at[0])
     forward((0, 1), (1,))
     first.relay(1)
-    spread((2,))
     forward((0, 1), (2,))
     first.cross(1)
+    spread((2,))
     first.normalise(1, gain_one, normed.at[1])
     arrive(extra.at[at.near], extra_sems.at[at.near], {"fs": at.near})
     for moving, extra_part in local:
@@ -643,6 +643,18 @@
             (core_sems, x_sems, z_sems),
         )
 
+    def raised(k, columns):
+        product = jnp.dot(normed[k], up_w[:, columns], preferred_element_type=jnp.float32)
+        positive = jnp.maximum(product, 0.0)
+        squared[k, :, columns] = (positive * positive).astype(squared.dtype)
+
+    def lift(k):
+        raised(k, pl.ds(0, least))
+
+        @pl.when(at.is_inner)
+        def _():
+            raised(k, pl.ds(least, most - least))
+
     summed = scatter(0)
     mix(1)
     forward((2,), (2,))
@@ -657,14 +669,15 @@
     summed.x(0)
     summed.z(1)
     spread(DOWN[:1], (2, 3, 1), at.is_inner)
-    forward(UP[:1])
     spread(DOWN[:1], (1,), at.is_outer)
+    forward(UP[:1], (1,))
     summed.own(tokens, residual)
 
     second = Gather(at, link, False, residual, held_two, arrived)
     second.begin()
     spread(DOWN[1:], (1,), at.is_outer)
     held_two[place, at.row] = residual[...]
+    forward(UP[:1], (2, 3))
     forward(UP[1:])
     forward(DOWN[:1], (1,))
     second.relay(1)
@@ -676,30 +689,21 @@
     second.cross(1)
     forward(DOWN[:1], (2,))
     second.normalise(0, gain_two, normed.at[0])
+    for number in UP:
+        weights.wait(number)
+    lift(0)
+    second.normalise(1, gain_two, normed.at[1])
+    lift(1)
     second.relay(3)
     second.cross(2)
     forward(DOWN[:1], (3,))
     forward(DOWN[1:], (2,))
-    second.normalise(1, gain_two, normed.at[1])
     second.normalise(2, gain_two, normed.at[2])
+    lift(2)
     second.cross(3)
     forward(DOWN[1:], (1,))
     second.normalise(3, gain_two, normed.at[3])
     forward(DOWN[1:], (3,))
-    for number in UP:
-        weights.wait(number)
-    def raised(k, columns):
-        product = jnp.dot(normed[k], up_w[:, columns], preferred_element_type=jnp.float32)
-        positive = jnp.maximum(product, 0.0)
-        squared[k, :, columns] = (positive * positive).astype(squared.dtype)
-
-    def lift(k):
-        raised(k, pl.ds(0, least))
-
-        @pl.when(at.is_inner)
-        def _():
-            raised(k, pl.ds(least, most - least))
-
     def lowered(k, count):
         for part in range(4):
             terms[1, k, part] = jnp.dot(
@@ -719,9 +723,6 @@
 
     last = scatter(1)
     lift(3)
-    lift(2)
-    lift(1)
-    lift(0)
     for number in DOWN:
         weights.wait(number)
     lower(3)
@@ -803,8 +804,8 @@
             dma((POOL,)),
             dma((4, 4, PIECES)),
             dma((2, 4)),
-            dma((4, PIECES)),
-            dma((5, PIECES)),
+            dma((4, SPLIT)),
+            dma((5, SPLIT)),
             dma((7, 2, 4)),
             dma((4,)),
             dma((7, 2)),

time: 138 us -> 136 us (0.986)
  no operation moved by 1% of the time
where the time goes in v4:
time: 136 us
  Pallas kernels  135 us (99%)
  local copies, waits for them, and re-layouts  1.67 us (1%)
    pallas_call x1, Pallas kernels, per_device_owned(): pl.pallas_call(layer_kernel, out_shape=jax.ShapeDtypeStruct(block, kind),...  135 us

profile of v4, /device:TPU:0, one launch (start us, length us, event | category | flops | bytes accessed | tf_op | source)
XLA Modules:
  0.0 136.3 jit_solution(2959190564585541261)
XLA Ops:
  0.0 134.6 %shard_map.127 = bf16[256,512]{1,0:T(8,128)(2,1)} custom-call(bf16[256,512]{1,0:T(8,128)(2,1)} %tokens_from.1, f32[1,2048]{1,0:T(1,128)} %bitcast.4, f32[1,2048]{1,0:T(1,128)} %bitcast.5, bf16[4,512]{1,0:T(4,128)(2,1)} %taps_from.1, bf16[4,128,128]{2,1,0:T(8,128)(2,1)} %decay_map_from.1, bf16[4,128,128]{2,1,0:T(8,128)(2,1)} %input_map_from.1, ...), custom_call_target="tpu_custom_call" | custom-call | tf_op jit(solution)/shard_map/pallas_call | solution.py:796
  134.7 1.7 %copy.15 = bf16[256,512]{1,0:T(8,128)(2,1)} copy(bf16[256,512]{1,0:T(8,128)(2,1)} %shard_map.127) | data formatting | bytes 524288
